TPU v7x, 32 devices: a whole 2x2x4 slice. The times are simulated.
32 devices in a mesh: rep: 2 (over x), fs: 8 (over z, y), tp: 2 (over core).
Axes of the slice: x: 2, y: 2, z: 4, core: 2. Of those that a mesh axis runs over, the one named last changes fastest.
Arguments:
- tokens: bfloat16 [8192, 2048], P(('rep', 'fs'), 'tp'), may hold values from -6 to 6
- mix_gain: float32 [2048], replicated, may hold values from 0.1 to 1.9
- query_w: bfloat16 [2048, 2048], P('fs', 'tp'), may hold values from -0.125 to 0.125
- key_w: bfloat16 [2048, 2048], P('fs', 'tp'), may hold values from -0.125 to 0.125
- value_w: bfloat16 [2048, 4096], P('fs', 'tp'), may hold values from -0.125 to 0.125
- head_gain: float32 [8, 512], replicated, may hold values from 0.1 to 1.9
- out_w: bfloat16 [4096, 2048], P('tp', 'fs'), may hold values from -0.09375 to 0.09375
- chan_gain: float32 [2048], replicated, may hold values from 0.1 to 1.9
- up_w: bfloat16 [2048, 4096], P('fs', 'tp'), may hold values from -0.125 to 0.125
- down_w: bfloat16 [4096, 2048], P('tp', 'fs'), may hold values from -0.09375 to 0.09375
Outputs:
- layer_out: bfloat16 [8192, 2048], P(('rep', 'fs'), 'tp')
All inputs are finite; a program needn't handle non-finite values.
Results may differ from a plain program's by a relative error of at most 0.019.
Values may be sent and summed in bfloat16 or wider, within the bound.
No kernel may reach another device: no remote copies, remote signals or barrier semaphores. Data moves between devices by JAX's collectives and lax.ppermute only.
A program may use at most 128 MiB of HBM per device.

v0:
```python
import jax
import jax.numpy as jnp
from jax import lax
from jax.sharding import PartitionSpec as P


DK = 256
DV = 512

EPS = 1e-06
HEAD_EPS = 0.05
THETA = 10000.0


def norm_rows(block, gain, tp, width):
    if tp == 2:
        other = swap(block, "tp")
        first = lax.axis_index("tp") == 0
        halves = [jnp.where(first, block, other), jnp.where(first, other, block)]
        whole = [block, other]
    else:
        halves = [lax.all_gather(block, "tp", axis=1, tiled=True)]
        whole = halves
    total = sum(
        jnp.sum(jnp.square(part.astype(jnp.float32)), axis=-1, keepdims=True) for part in whole
    )
    scale = lax.rsqrt(total / gain.shape[0] + EPS)
    span = halves[0].shape[1]
    blocks = [half[:, at : at + width] for half in halves for at in range(0, span, width)]
    gains = [gain[at : at + width] for at in range(0, gain.shape[0], width)]
    return tuple(
        (rows.astype(jnp.float32) * scale * part).astype(jnp.bfloat16)
        for rows, part in zip(unweave(blocks), unweave(gains))
    )


def swap(x, axis):
    return lax.ppermute(x, axis, [(0, 1), (1, 0)])


def sum_parts(x, axis, size, dim):
    if size == 1:
        return x
    if size != 2:
        return lax.psum_scatter(
            x.astype(jnp.bfloat16), axis, scatter_dimension=dim, tiled=True
        ).astype(jnp.float32)
    part = x.shape[dim] // 2
    me = lax.axis_index(axis)
    away = lax.dynamic_slice_in_dim(x, (1 - me) * part, part, dim).astype(jnp.bfloat16)
    kept = lax.dynamic_slice_in_dim(x, me * part, part, dim)
    return kept + swap(away, axis).astype(jnp.float32)


def gather_fs(x, dim, size):
    groups = [list(range(0, size, 2)), list(range(1, size, 2))]
    return lax.all_gather(x, "fs", axis=dim, tiled=True, axis_index_groups=groups)


def cross(x, size):
    return lax.ppermute(x, "fs", [(i, i ^ 1) for i in range(size)])


def even():
    return lax.axis_index("fs") % 2 == 0


def unweave(blocks):
    mine = [jnp.where(even(), a, b) for a, b in zip(blocks[::2], blocks[1::2])]
    other = [jnp.where(even(), b, a) for a, b in zip(blocks[::2], blocks[1::2])]
    return jnp.concatenate(mine, axis=-1), jnp.concatenate(other, axis=-1)


def weave(mine, other, width):
    first = jnp.where(even(), mine, other)
    second = jnp.where(even(), other, mine)
    pieces = []
    for at in range(0, mine.shape[1], width):
        pieces += [first[:, at : at + width], second[:, at : at + width]]
    return jnp.concatenate(pieces, axis=1)


def share(x, count, dim):
    if count == 1:
        return x
    part = x.shape[dim] // count
    return lax.dynamic_slice_in_dim(x, lax.axis_index("rep") * part, part, dim)


def rotate(field, cosine, sine):
    half = field.shape[-1] // 2
    first = field[:, :half]
    second = field[:, half:]
    return jnp.concatenate(
        [first * cosine - second * sine, second * cosine + first * sine], axis=-1
    )


def make(mesh):
    tp = mesh.shape["tp"]
    rep = mesh.shape["rep"]
    fs = mesh.shape["fs"]

    def layer_body(
        tokens, mix_gain, query_w, key_w, value_w, head_gain, out_w, chan_gain, up_w, down_w
    ):
        rows = tokens.shape[0]
        local = query_w.shape[1] // DK
        pair = rep == 2
        split_heads = 2 if pair and local % 2 == 0 else 1
        split_units = 2 if pair and up_w.shape[1] % 256 == 0 else 1
        heads = local // split_heads

        width = query_w.shape[0]
        down_part = share(down_w, split_units, 0)
        down_other = cross(down_part, fs)
        qk_w = jnp.concatenate(
            [share(query_w, split_heads, 1), share(key_w, split_heads, 1)], axis=1
        )
        qk_mine = gather_fs(qk_w, 0, fs)
        value_mine = gather_fs(share(value_w, split_heads, 1), 0, fs)
        out_mine = gather_fs(share(out_w, split_heads, 0), 1, fs)
        up_mine = gather_fs(share(up_w, split_units, 1), 0, fs)
        down_full = gather_fs(weave(down_part, down_other, down_part.shape[1]), 1, fs)
        qk_other = cross(qk_mine, fs)
        value_other = cross(value_mine, fs)
        out_other = cross(out_mine, fs)
        up_other = cross(up_mine, fs)

        def product(rows, mine, other):
            return jnp.dot(rows[0], mine, preferred_element_type=jnp.float32) + jnp.dot(
                rows[1], other, preferred_element_type=jnp.float32
            )

        first_head = lax.axis_index("tp") * local
        if split_heads == 2:
            first_head = first_head + lax.axis_index("rep") * heads
        numbers = (first_head + jnp.arange(heads, dtype=jnp.int32)).astype(jnp.float32)
        log_rate = jnp.log1p(-jnp.exp2(-5.0 - numbers))
        gains = lax.dynamic_slice_in_dim(head_gain, first_head, heads, 0)

        places = jnp.arange(rows, dtype=jnp.int32).astype(jnp.float32)
        inverse = THETA ** (-jnp.arange(DK // 2, dtype=jnp.float32) / (DK // 2))
        angles = places[:, None] * inverse
        cosine, sine = jnp.cos(angles), jnp.sin(angles)
        offset = places[:, None] - places[None, :]
        masks = [
            jnp.where(offset >= 0, jnp.exp(log_rate[h] * jnp.maximum(offset, 0.0)), 0.0)
            for h in range(heads)
        ]

        def mixer_terms(block):
            normed = norm_rows(block, mix_gain, tp, width)
            raw = product(normed, qk_mine, qk_other)
            vraw = product(normed, value_mine, value_other).astype(jnp.bfloat16)
            outs = []
            for h in range(heads):
                query = rotate(raw[:, h * DK : (h + 1) * DK], cosine, sine).astype(jnp.bfloat16)
                at = heads * DK + h * DK
                keys = (rotate(raw[:, at : at + DK], cosine, sine) * DK ** (-0.5)).astype(
                    jnp.bfloat16
                )
                values = vraw[:, h * DV : (h + 1) * DV]
                scores = lax.dot_general(
                    query, keys, (((1,), (1,)), ((), ())), preferred_element_type=jnp.float32
                )
                weights = (scores * masks[h]).astype(jnp.bfloat16)
                kept = jnp.dot(weights, values, preferred_element_type=jnp.float32)
                scale = lax.rsqrt(jnp.mean(kept * kept, axis=-1, keepdims=True) + HEAD_EPS)
                outs.append((kept * scale * gains[h]).astype(jnp.bfloat16))
            head_out = jnp.concatenate(outs, axis=1)
            terms = [
                jnp.dot(head_out, part, preferred_element_type=jnp.float32)
                for part in (out_mine, out_other)
            ]
            if tp == 2 and (fs // tp) % 2 == 0:
                terms = [sum_parts(part, "tp", tp, 1) for part in terms]
                return terms
            return [sum_parts(weave(*terms, out_w.shape[1]), "tp", tp, 1)]

        def chan_terms(block):
            normed = norm_rows(block, chan_gain, tp, width)
            upward = product(normed, up_mine, up_other)
            hidden = jnp.square(jax.nn.relu(upward)).astype(jnp.bfloat16)
            terms = jnp.dot(hidden, down_full, preferred_element_type=jnp.float32)
            return [sum_parts(terms, "tp", tp, 1)]

        def layer(block, terms, split):
            if split == 1:
                total = terms(block)
            else:
                away = [part.astype(jnp.bfloat16) for part in terms(swap(block, "rep"))]
                back = [swap(part, "rep").astype(jnp.float32) for part in away]
                total = [part + more for part, more in zip(terms(block), back)]
            if len(total) == 2:
                total = [weave(*total, out_w.shape[1])]
            return (block.astype(jnp.float32) + total[0]).astype(jnp.bfloat16)

        middle = layer(tokens, mixer_terms, split_heads)
        return layer(middle, chan_terms, split_units)

    return layer_body


def solution(mesh):
    placed = (
        P(("rep", "fs"), "tp"),
        P(),
        P("fs", "tp"),
        P("fs", "tp"),
        P("fs", "tp"),
        P(),
        P("tp", "fs"),
        P(),
        P("fs", "tp"),
        P("tp", "fs"),
    )
    return jax.shard_map(
        make(mesh), mesh=mesh, in_specs=placed, out_specs=P(("rep", "fs"), "tp"), check_vma=False
    )
```

profile of v0, /device:TPU:0, one launch (start us, length us, event | category | flops | bytes accessed | tf_op | source)
XLA Modules:
  0.0 351.2 jit_solution(12954669410991172848)
XLA Ops:
  21.9 9.8 %collective-permute-done.14 = bf16[1024,256]{1,0:T(8,128)(2,1)} collective-permute-done((bf16[1024,256]{1,0:T(8,128)(2,1)}, bf16[1024,256]{1,0:T(8,128)(2,1)}, u32[]{:S(2)}, u32[]{:S(2)}) %collective-permute-start.14) | collective-permute-done | bytes 524320 | tf_op jit(solution)/shard_map/ppermute | solution.py:61
  34.2 5.1 %collective-permute-done.4 = bf16[512,1024]{1,0:T(8,128)(2,1)S(1)} collective-permute-done((bf16[512,1024]{1,0:T(8,128)(2,1)S(1)}, bf16[512,1024]{1,0:T(8,128)(2,1)S(1)}, u32[]{:S(2)}, u32[]{:S(2)}) %collective-permute-start.4) | collective-permute-done | bytes 1048608 | tf_op jit(solution)/shard_map/ppermute | solution.py:38
  43.0 15.1 %all-gather.6.cloned.1.call-done = bf16[1024,1024]{1,0:T(8,128)(2,1)} async-done(((bf16[256,1024]{1,0:T(8,128)(2,1)}), bf16[1024,1024]{1,0:T(8,128)(2,1)}) %all-gather.6.cloned.1.call-update) | async-done | bytes 2097168 | tf_op jit(solution)/shard_map/all_gather | solution.py:57
  61.5 42.6 %all-gather.8.cloned.1.call-done = bf16[1024,1024]{1,0:T(8,128)(2,1)} async-done(((bf16[256,1024]{1,0:T(8,128)(2,1)}), bf16[1024,1024]{1,0:T(8,128)(2,1)}) %all-gather.8.cloned.1.call-update) | async-done | bytes 2097168 | tf_op jit(solution)/shard_map/all_gather | solution.py:57
  105.6 45.2 %all-gather.10.cloned.1.call-done = bf16[1024,1024]{1,0:T(8,128)(2,1)} async-done(((bf16[1024,256]{1,0:T(8,128)(2,1)}), bf16[1024,1024]{1,0:T(8,128)(2,1)}) %all-gather.10.cloned.1.call-update) | async-done | bytes 2097168 | tf_op jit(solution)/shard_map/all_gather | solution.py:57
  152.3 3.4 fusion.226
  160.5 2.7 fusion.229
  163.2 2.9 convolution_add_fusion.1
  168.6 3.9 %add_convert_fusion.2 = bf16[512,1024]{1,0:T(8,128)(2,1)} fusion(f32[512,1024]{1,0:T(8,128)S(1)} %fusion.226, bf16[1024,1024]{1,0:T(8,128)(2,1)} %collective-permute-done.2, bf16[512,256]{1,0:T(8,128)(2,1)S(1)} %copy-done.9, bf16[512,256]{1,0:T(8,128)(2,1)S(1)} %get-tuple-element.59, bf16[512,256]{1,0:T(8,128)(2,1)S(1)} %copy-done.13, ...), kind=kOutput, calls=%fused_computation.25 | convolution fusion | flops 1080557568 | bytes 6297600 | tf_op jit(solution)/shard_map/dot_general | solution.py:131
  172.5 4.4 %multiply_reduce_fusion.8 = (f32[512]{0:T(512)}, f32[512,512]{0,1:T(8,128)}) fusion(bf16[512,1024]{1,0:T(8,128)(2,1)} %add_convert_fusion.2, f32[]{:T(128)} %bitcast.2, f32[512]{0:T(512)S(1)} %iota_convert_fusion, f32[512,128]{1,0:T(8,128)} %get-tuple-element.11, f32[512,128]{1,0:T(8,128)} %get-tuple-element.10, bf16[512,128]{1,0:T(8,128)(2,1)} %get-tuple-element.13, ...), kind=kOutput, calls=%fused_computation.105 | convolution fusion | flops 405929472 | bytes 2365952 | tf_op jit(solution)/shard_map/dot_general | solution.py:168
  177.7 3.8 %convolution_add_fusion = f32[512,1024]{1,0:T(8,128)S(1)} fusion(f32[512,1024]{1,0:T(8,128)} %fusion.229, bf16[1024,1024]{1,0:T(8,128)(2,1)} %collective-permute-done.1, bf16[512,256]{1,0:T(8,128)(2,1)} %get-tuple-element.70, bf16[512,256]{1,0:T(8,128)(2,1)S(1)} %copy-done.10, bf16[512,256]{1,0:T(8,128)(2,1)} %get-tuple-element.66, ...), kind=kOutput, calls=%fused_computation.31 | convolution fusion | flops 1080033280 | bytes 7346176 | tf_op jit(solution)/shard_map/dot_general | solution.py:131
  183.9 4.0 %add_convert_fusion.1 = bf16[512,1024]{1,0:T(8,128)(2,1)} fusion(f32[512,1024]{1,0:T(8,128)S(1)} %copy-done.43, bf16[1024,1024]{1,0:T(8,128)(2,1)} %collective-permute-done.2, bf16[512,256]{1,0:T(8,128)(2,1)S(1)} %copy-done.11, bf16[512,256]{1,0:T(8,128)(2,1)S(1)} %copy-done.10, bf16[512,256]{1,0:T(8,128)(2,1)S(1)} %copy-done.15, ...), kind=kOutput, calls=%fused_computation.20 | convolution fusion | flops 1080557568 | bytes 6297600 | tf_op jit(solution)/shard_map/dot_general | solution.py:131
  187.9 4.4 %multiply_reduce_fusion.6 = (f32[512]{0:T(512)}, f32[512,512]{0,1:T(8,128)}) fusion(bf16[512,1024]{1,0:T(8,128)(2,1)} %add_convert_fusion.1, f32[]{:T(128)} %bitcast.2, f32[512]{0:T(512)S(1)} %iota_convert_fusion, f32[512,128]{1,0:T(8,128)} %get-tuple-element.19, f32[512,128]{1,0:T(8,128)} %get-tuple-element.18, bf16[512,128]{1,0:T(8,128)(2,1)} %get-tuple-element.21, ...), kind=kOutput, calls=%fused_computation.100 | convolution fusion | flops 405929472 | bytes 2365952 | tf_op jit(solution)/shard_map/dot_general | solution.py:168
  193.0 4.3 %multiply_reduce_fusion.9 = (f32[512]{0:T(512)}, f32[512,512]{0,1:T(8,128)}) fusion(bf16[512,1024]{1,0:T(8,128)(2,1)} %add_convert_fusion.2, f32[]{:T(128)} %bitcast, f32[512]{0:T(512)S(1)} %iota_convert_fusion, f32[512,128]{1,0:T(8,128)} %get-tuple-element.15, f32[512,128]{1,0:T(8,128)S(1)} %copy-done.16, bf16[512,128]{1,0:T(8,128)(2,1)} %get-tuple-element.16, ...), kind=kOutput, calls=%fused_computation.107 | convolution fusion | flops 405929472 | bytes 2365952 | tf_op jit(solution)/shard_map/dot_general | solution.py:168
  198.0 3.8 %multiply_reduce_fusion.7 = (f32[512]{0:T(512)S(1)}, f32[512,512]{0,1:T(8,128)}) fusion(bf16[512,1024]{1,0:T(8,128)(2,1)} %add_convert_fusion.1, f32[]{:T(128)} %bitcast, f32[512]{0:T(512)S(1)} %iota_convert_fusion, f32[512,128]{1,0:T(8,128)} %get-tuple-element.23, f32[512,128]{1,0:T(8,128)} %get-tuple-element.22, bf16[512,128]{1,0:T(8,128)(2,1)} %get-tuple-element.24, ...), kind=kOutput, calls=%fused_computation.102 | convolution fusion | flops 405929472 | bytes 2365952 | tf_op jit(solution)/shard_map/dot_general | solution.py:168
  215.2 12.5 %collective-permute-done.7 = bf16[512,512]{1,0:T(8,128)(2,1)S(1)} collective-permute-done((bf16[512,512]{1,0:T(8,128)(2,1)S(1)}, bf16[512,512]{1,0:T(8,128)(2,1)S(1)}, u32[]{:S(2)}, u32[]{:S(2)}) %collective-permute-start.7) | collective-permute-done | bytes 524320 | tf_op jit(solution)/shard_map/ppermute | solution.py:38
  227.7 10.3 %collective-permute-done.11 = bf16[512,512]{1,0:T(8,128)(2,1)S(1)} collective-permute-done((bf16[512,512]{1,0:T(8,128)(2,1)S(1)}, bf16[512,512]{1,0:T(8,128)(2,1)S(1)}, u32[]{:S(2)}, u32[]{:S(2)}) %collective-permute-start.11) | collective-permute-done | bytes 524320 | tf_op jit(solution)/shard_map/ppermute | solution.py:38
  240.9 22.6 %collective-permute-done.16 = bf16[512,1024]{1,0:T(8,128)(2,1)S(1)} collective-permute-done((bf16[512,1024]{1,0:T(8,128)(2,1)S(1)}, bf16[512,1024]{1,0:T(8,128)(2,1)S(1)}, u32[]{:S(2)}, u32[]{:S(2)}) %collective-permute-start.16) | collective-permute-done | bytes 1048608 | tf_op jit(solution)/shard_map/ppermute | solution.py:38
  268.1 3.0 fusion.23
  271.1 17.8 %collective-permute-done.13 = bf16[1024,1024]{1,0:T(8,128)(2,1)} collective-permute-done((bf16[1024,1024]{1,0:T(8,128)(2,1)}, bf16[1024,1024]{1,0:T(8,128)(2,1)}, u32[]{:S(2)}, u32[]{:S(2)}) %collective-permute-start.13) | collective-permute-done | bytes 2097184 | tf_op jit(solution)/shard_map/ppermute | solution.py:61
  289.0 8.9 %fusion.61 = f32[512,2048]{1,0:T(8,128)} fusion(bf16[1024,2048]{1,0:T(8,128)(2,1)} %all-gather.14.cloned.1.call-done, f32[512,1024]{1,0:T(8,128)} %fusion.23, bf16[1024,1024]{1,0:T(8,128)(2,1)} %collective-permute-done.13, bf16[512,256]{1,0:T(8,128)(2,1)S(1)} %get-tuple-element.48, bf16[512,256]{1,0:T(8,128)(2,1)S(1)} %get-tuple-element.45, ...), kind=kOutput, calls=%fused_computation.117 | convolution fusion | flops 3229089792 | bytes 13637632 | tf_op jit(solution)/shard_map/dot_general | solution.py:185
  299.9 4.2 %fusion.22 = f32[512,1024]{1,0:T(8,128)} fusion(bf16[1024,1024]{1,0:T(8,128)(2,1)} %all-gather.12.cloned.1.call-done, bf16[512,256]{1,0:T(8,128)(2,1)S(1)} %copy-done.18, bf16[512,256]{1,0:T(8,128)(2,1)S(1)} %copy-done.17, bf16[512,256]{1,0:T(8,128)(2,1)S(1)} %copy-done.19, bf16[512,256]{1,0:T(8,128)(2,1)S(1)} %copy-done.20, ...), kind=kOutput, calls=%fused_computation.51 | convolution fusion | flops 1079508992 | bytes 5249024 | tf_op jit(solution)/shard_map/dot_general | solution.py:131
  304.1 9.2 %fusion.60 = f32[512,2048]{1,0:T(8,128)} fusion(bf16[1024,2048]{1,0:T(8,128)(2,1)} %all-gather.14.cloned.1.call-done, f32[512,1024]{1,0:T(8,128)} %fusion.22, bf16[1024,1024]{1,0:T(8,128)(2,1)} %collective-permute-done.13, bf16[512,256]{1,0:T(8,128)(2,1)} %get-tuple-element.40, bf16[512,256]{1,0:T(8,128)(2,1)S(1)} %get-tuple-element.37, ...), kind=kOutput, calls=%fused_computation.116 | convolution fusion | flops 3229089792 | bytes 13637632 | tf_op jit(solution)/shard_map/dot_general | solution.py:185
  318.6 24.3 %collective-permute-done.19 = bf16[512,1024]{1,0:T(8,128)(2,1)S(1)} collective-permute-done((bf16[512,1024]{1,0:T(8,128)(2,1)S(1)}, bf16[512,1024]{1,0:T(8,128)(2,1)S(1)}, u32[]{:S(2)}, u32[]{:S(2)}) %collective-permute-start.19) | collective-permute-done | bytes 1048608 | tf_op jit(solution)/shard_map/ppermute | solution.py:38
  (202 shorter events, 69.0 us)
Async XLA Ops:
  6.5 51.5 %all-gather.6.cloned.1.call-start = ((), (), s32[]{:S(2)}) async-start(), calls=%async_computation | async-start | bytes 2621440 | tf_op jit(solution)/shard_map/all_gather | solution.py:57
  9.5 94.6 %all-gather.8.cloned.1.call-start = ((), (), s32[]{:S(2)}) async-start(), calls=%async_computation.1 | async-start | bytes 2621440 | tf_op jit(solution)/shard_map/all_gather | solution.py:57
  10.5 140.3 %all-gather.10.cloned.1.call-start = ((), (), s32[]{:S(2)}) async-start(), calls=%async_computation.2 | async-start | bytes 2621440 | tf_op jit(solution)/shard_map/all_gather | solution.py:57
  11.4 229.1 %all-gather.12.cloned.1.call-start = ((), (), s32[]{:S(2)}) async-start(), calls=%async_computation.3 | async-start | bytes 2621440 | tf_op jit(solution)/shard_map/all_gather | solution.py:57
  12.4 276.6 %all-gather.14.cloned.1.call-start = ((), (), s32[]{:S(2)}) async-start(), calls=%async_computation.4 | async-start | bytes 5242880 | tf_op jit(solution)/shard_map/all_gather | solution.py:57
  12.4 27.2 %collective-permute-start = (bf16[512,1024]{1,0:T(8,128)(2,1)S(1)}, bf16[512,1024]{1,0:T(8,128)(2,1)S(1)}, u32[]{:S(2)}, u32[]{:S(2)}) collective-permute-start(bf16[512,1024]{1,0:T(8,128)(2,1)S(1)} %copy-done.2), channel_id=1, source_target_pairs={{0,1},{1,0},{2,3},{3,2},{4,5},{5,4},{6,7},{7,6},{8,9},{9,8},{10,11... | collective-permute-start | bytes 3145736 | tf_op jit(solution)/shard_map/ppermute | solution.py:38
  13.0 26.3 %collective-permute-start.4 = (bf16[512,1024]{1,0:T(8,128)(2,1)S(1)}, bf16[512,1024]{1,0:T(8,128)(2,1)S(1)}, u32[]{:S(2)}, u32[]{:S(2)}) collective-permute-start(bf16[512,1024]{1,0:T(8,128)(2,1)S(1)} %copy-done.2), channel_id=1, source_target_pairs={{0,16},{16,0},{1,17},{17,1},{2,18},{18,2},{3,19},{19,3},{4,20},{20... | collective-permute-start | bytes 3145736 | tf_op jit(solution)/shard_map/ppermute | solution.py:38
  17.4 14.3 %collective-permute-start.14 = (bf16[1024,256]{1,0:T(8,128)(2,1)}, bf16[1024,256]{1,0:T(8,128)(2,1)}, u32[]{:S(2)}, u32[]{:S(2)}) collective-permute-start(bf16[1024,256]{1,0:T(8,128)(2,1)} %constant_dynamic-slice_fusion.1), channel_id=1, source_target_pairs={{0,2},{2,0},{4,6},{6,4},{8,10},{10,8},{12,14},{14,12},{1,3},{3,1},... | collective-permute-start | bytes 1572872 | tf_op jit(solution)/shard_map/ppermute | solution.py:61
  39.3 3.0 collective-permute-start.5
  58.1 105.1 %collective-permute-start.1 = (bf16[1024,1024]{1,0:T(8,128)(2,1)}, bf16[1024,1024]{1,0:T(8,128)(2,1)}, u32[]{:S(2)}, u32[]{:S(2)}) collective-permute-start(bf16[1024,1024]{1,0:T(8,128)(2,1)} %all-gather.6.cloned.1.call-done), channel_id=1, source_target_pairs={{0,2},{2,0},{4,6},{6,4},{8,10},{10,8},{12,14},{14,12},{1,3},{3,1},... | collective-permute-start | bytes 6291464 | tf_op jit(solution)/shard_map/ppermute | solution.py:61
  104.1 64.5 %collective-permute-start.2 = (bf16[1024,1024]{1,0:T(8,128)(2,1)}, bf16[1024,1024]{1,0:T(8,128)(2,1)}, u32[]{:S(2)}, u32[]{:S(2)}) collective-permute-start(bf16[1024,1024]{1,0:T(8,128)(2,1)} %all-gather.8.cloned.1.call-done), channel_id=1, source_target_pairs={{0,2},{2,0},{4,6},{6,4},{8,10},{10,8},{12,14},{14,12},{1,3},{3,1},... | collective-permute-start | bytes 6291464 | tf_op jit(solution)/shard_map/ppermute | solution.py:61
  150.8 58.4 %collective-permute-start.8 = (bf16[1024,1024]{1,0:T(8,128)(2,1)}, bf16[1024,1024]{1,0:T(8,128)(2,1)S(1)}, u32[]{:S(2)}, u32[]{:S(2)}) collective-permute-start(bf16[1024,1024]{1,0:T(8,128)(2,1)} %all-gather.10.cloned.1.call-done), channel_id=1, source_target_pairs={{0,2},{2,0},{4,6},{6,4},{8,10},{10,8},{12,14},{14,12},{1,3},{3,1},... | collective-permute-start | bytes 6291464 | tf_op jit(solution)/shard_map/ppermute | solution.py:61
  207.2 5.4 %collective-permute-start.6 = (bf16[512,512]{1,0:T(8,128)(2,1)S(1)}, bf16[512,512]{1,0:T(8,128)(2,1)S(1)}, u32[]{:S(2)}, u32[]{:S(2)}) collective-permute-start(bf16[512,512]{1,0:T(8,128)(2,1)S(1)} %dynamic-slice_convert_fusion.4), channel_id=1, source_target_pairs={{0,1},{1,0},{2,3},{3,2},{4,5},{5,4},{6,7},{7,6},{8,9},{9,8},{10,11... | collective-permute-start | bytes 1572872 | tf_op jit(solution)/shard_map/ppermute | solution.py:38
  208.6 6.5 %collective-permute-start.3 = (bf16[512,512]{1,0:T(8,128)(2,1)S(1)}, bf16[512,512]{1,0:T(8,128)(2,1)S(1)}, u32[]{:S(2)}, u32[]{:S(2)}) collective-permute-start(bf16[512,512]{1,0:T(8,128)(2,1)S(1)} %dynamic-slice_convert_fusion.5), channel_id=1, source_target_pairs={{0,1},{1,0},{2,3},{3,2},{4,5},{5,4},{6,7},{7,6},{8,9},{9,8},{10,11... | collective-permute-start | bytes 1572872 | tf_op jit(solution)/shard_map/ppermute | solution.py:38
  210.6 3.6 %collective-permute-start.10 = (bf16[512,512]{1,0:T(8,128)(2,1)S(1)}, bf16[512,512]{1,0:T(8,128)(2,1)S(1)}, u32[]{:S(2)}, u32[]{:S(2)}) collective-permute-start(bf16[512,512]{1,0:T(8,128)(2,1)S(1)} %dynamic-slice_convert_fusion.2), channel_id=1, source_target_pairs={{0,1},{1,0},{2,3},{3,2},{4,5},{5,4},{6,7},{7,6},{8,9},{9,8},{10,11... | collective-permute-start | bytes 1572872 | tf_op jit(solution)/shard_map/ppermute | solution.py:38
  212.1 3.1 collective-permute-start.9
  212.8 14.9 %collective-permute-start.7 = (bf16[512,512]{1,0:T(8,128)(2,1)S(1)}, bf16[512,512]{1,0:T(8,128)(2,1)S(1)}, u32[]{:S(2)}, u32[]{:S(2)}) collective-permute-start(bf16[512,512]{1,0:T(8,128)(2,1)S(1)} %add_convert_fusion.4), channel_id=1, source_target_pairs={{0,16},{16,0},{1,17},{17,1},{2,18},{18,2},{3,19},{19,3},{4,20},{20... | collective-permute-start | bytes 1572872 | tf_op jit(solution)/shard_map/ppermute | solution.py:38
  214.4 23.5 %collective-permute-start.11 = (bf16[512,512]{1,0:T(8,128)(2,1)S(1)}, bf16[512,512]{1,0:T(8,128)(2,1)S(1)}, u32[]{:S(2)}, u32[]{:S(2)}) collective-permute-start(bf16[512,512]{1,0:T(8,128)(2,1)S(1)} %add_convert_fusion.3), channel_id=1, source_target_pairs={{0,16},{16,0},{1,17},{17,1},{2,18},{18,2},{3,19},{19,3},{4,20},{20... | collective-permute-start | bytes 1572872 | tf_op jit(solution)/shard_map/ppermute | solution.py:38
  239.0 24.4 %collective-permute-start.16 = (bf16[512,1024]{1,0:T(8,128)(2,1)S(1)}, bf16[512,1024]{1,0:T(8,128)(2,1)S(1)}, u32[]{:S(2)}, u32[]{:S(2)}) collective-permute-start(bf16[512,1024]{1,0:T(8,128)(2,1)S(1)} %get-tuple-element.6), channel_id=1, source_target_pairs={{0,16},{16,0},{1,17},{17,1},{2,18},{18,2},{3,19},{19,3},{4,20},{20... | collective-permute-start | bytes 3145736 | tf_op jit(solution)/shard_map/ppermute | solution.py:38
  240.5 23.0 %collective-permute-start.12 = (bf16[512,1024]{1,0:T(8,128)(2,1)S(1)}, bf16[512,1024]{1,0:T(8,128)(2,1)S(1)}, u32[]{:S(2)}, u32[]{:S(2)}) collective-permute-start(bf16[512,1024]{1,0:T(8,128)(2,1)S(1)} %get-tuple-element.6), channel_id=1, source_target_pairs={{0,1},{1,0},{2,3},{3,2},{4,5},{5,4},{6,7},{7,6},{8,9},{9,8},{10,11... | collective-permute-start | bytes 3145736 | tf_op jit(solution)/shard_map/ppermute | solution.py:38
  240.5 48.4 %collective-permute-start.13 = (bf16[1024,1024]{1,0:T(8,128)(2,1)}, bf16[1024,1024]{1,0:T(8,128)(2,1)}, u32[]{:S(2)}, u32[]{:S(2)}) collective-permute-start(bf16[1024,1024]{1,0:T(8,128)(2,1)} %all-gather.12.cloned.1.call-done), channel_id=1, source_target_pairs={{0,2},{2,0},{4,6},{6,4},{8,10},{10,8},{12,14},{14,12},{1,3},{3,1},... | collective-permute-start | bytes 6291464 | tf_op jit(solution)/shard_map/ppermute | solution.py:61
  299.8 15.9 %collective-permute-start.18 = (bf16[512,1024]{1,0:T(8,128)(2,1)S(1)}, bf16[512,1024]{1,0:T(8,128)(2,1)S(1)}, u32[]{:S(2)}, u32[]{:S(2)}) collective-permute-start(bf16[512,1024]{1,0:T(8,128)(2,1)S(1)} %dynamic-slice_convert_fusion), channel_id=1, source_target_pairs={{0,1},{1,0},{2,3},{3,2},{4,5},{5,4},{6,7},{7,6},{8,9},{9,8},{10,11... | collective-permute-start | bytes 3145736 | tf_op jit(solution)/shard_map/ppermute | solution.py:38
  315.1 3.5 collective-permute-start.15
  317.8 25.1 %collective-permute-start.19 = (bf16[512,1024]{1,0:T(8,128)(2,1)S(1)}, bf16[512,1024]{1,0:T(8,128)(2,1)S(1)}, u32[]{:S(2)}, u32[]{:S(2)}) collective-permute-start(bf16[512,1024]{1,0:T(8,128)(2,1)S(1)} %add_convert_fusion), channel_id=1, source_target_pairs={{0,16},{16,0},{1,17},{17,1},{2,18},{18,2},{3,19},{19,3},{4,20},{20... | collective-permute-start | bytes 3145736 | tf_op jit(solution)/shard_map/ppermute | solution.py:38
  (45 other events, 409.4 us)
Sparse Core Ops, SparseCore 0:
  9.7 48.3 all-gather.5
  59.6 44.4 all-gather.7
  105.7 45.0 all-gather.9
  152.2 43.8 all-gather.11
  197.5 79.5 all-gather.13
where the time goes:
time: 352 us; the launch traced here: 351 us
  waiting for transfers between devices  206 us (59%)
  matrix products  72.2 us (21%)
  other arithmetic  26.3 us (7%)
  local copies, waits for them, and re-layouts  16.9 us (5%)
  starting transfers between devices  15.8 us (4%)
  between operations  13.8 us (4%)
    all_gather x5, waiting for transfers between devices, gather_fs(): lax.all_gather(x, 'fs', axis=dim, tiled=True, axis_index_groups=groups)  103 us
    ppermute x15, waiting for transfers between devices, swap(): return lax.ppermute(x, axis, [(0, 1), (1, 0)])  75.5 us
    ppermute x5, waiting for transfers between devices, cross(): return lax.ppermute(x, 'fs', [(i, i ^ 1) for i in range(size)])  27.7 us
    dot_general x2, matrix products, chan_terms(): terms = jnp.dot(hidden, down_full, preferred_element_type=jnp.float32)  18.2 us
    dot_general x6, matrix products, product(): jnp.dot(rows[0], mine, preferred_element_type=jnp.float32)  17.2 us
    dot_general x4, matrix products, mixer_terms(): kept = jnp.dot(weights, values, preferred_element_type=jnp.float32)  17 us
    dot_general x4, matrix products, product(): jnp.dot(rows[1], other, preferred_element_type=jnp.float32)  14.6 us
    ppermute x15, starting transfers between devices, swap(): return lax.ppermute(x, axis, [(0, 1), (1, 0)])  9.32 us
  transfers between devices with their start and end apart: 25, of which 11 were waited for; matrix products, arithmetic and copies ran while one was open for 27% of the time, Pallas kernels for 0%

commit v1 on v0

--- a/solution.py
+++ b/solution.py
@@ -149,7 +149,7 @@
             for h in range(heads)
         ]
 
-        def mixer_terms(block):
+        def mixer_terms(block, after=None):
             normed = norm_rows(block, mix_gain, tp, width)
             raw = product(normed, qk_mine, qk_other)
             vraw = product(normed, value_mine, value_other).astype(jnp.bfloat16)
@@ -178,10 +178,12 @@
                 return terms
             return [sum_parts(weave(*terms, out_w.shape[1]), "tp", tp, 1)]
 
-        def chan_terms(block):
+        def chan_terms(block, after=None):
             normed = norm_rows(block, chan_gain, tp, width)
             upward = product(normed, up_mine, up_other)
             hidden = jnp.square(jax.nn.relu(upward)).astype(jnp.bfloat16)
+            if after is not None:
+                hidden, after = lax.optimization_barrier((hidden, after))
             terms = jnp.dot(hidden, down_full, preferred_element_type=jnp.float32)
             return [sum_parts(terms, "tp", tp, 1)]
 
@@ -191,7 +193,7 @@
             else:
                 away = [part.astype(jnp.bfloat16) for part in terms(swap(block, "rep"))]
                 back = [swap(part, "rep").astype(jnp.float32) for part in away]
-                total = [part + more for part, more in zip(terms(block), back)]
+                total = [part + more for part, more in zip(terms(block, away[0]), back)]
             if len(total) == 2:
                 total = [weave(*total, out_w.shape[1])]
             return (block.astype(jnp.float32) + total[0]).astype(jnp.bfloat16)

time: 352 us -> 365 us (1.037)
  waiting for transfers between devices: 206 us -> 227 us
  matrix products: 72.2 us -> 65.1 us
    ppermute x5, waiting for transfers between devices: 27.7 us -> 48.8 us  [cross(): return lax.ppermute(x, 'fs', [(i, i ^ 1) for i in range(size)])]
    dot_general x2, matrix products: 18.2 us -> 11.4 us  [chan_terms(): terms = jnp.dot(hidden, down_full, preferred_element_type=jnp.float32)]
    dot_general x4 -> x5, matrix products: 14.6 us -> 17.6 us  [product(): jnp.dot(rows[1], other, preferred_element_type=jnp.float32)]
  transfers between devices with their start and end apart: 25 -> 25, of which waited for: 11 -> 12; matrix products, arithmetic and copies ran while one was open for 27% -> 23% of each run, Pallas kernels for 0% -> 0%
where the time goes in v1:
time: 365 us; the launch traced here: 364 us
  waiting for transfers between devices  227 us (62%)
  matrix products  65.1 us (18%)
  other arithmetic  25.6 us (7%)
  starting transfers between devices  16.4 us (4%)
  local copies, waits for them, and re-layouts  15.7 us (4%)
  between operations  13.9 us (4%)
    all_gather x5, waiting for transfers between devices, gather_fs(): lax.all_gather(x, 'fs', axis=dim, tiled=True, axis_index_groups=groups)  104 us
    ppermute x15, waiting for transfers between devices, swap(): return lax.ppermute(x, axis, [(0, 1), (1, 0)])  74.9 us
    ppermute x5, waiting for transfers between devices, cross(): return lax.ppermute(x, 'fs', [(i, i ^ 1) for i in range(size)])  48.8 us
    dot_general x5, matrix products, product(): jnp.dot(rows[1], other, preferred_element_type=jnp.float32)  17.6 us
    dot_general x4, matrix products, mixer_terms(): kept = jnp.dot(weights, values, preferred_element_type=jnp.float32)  16.8 us
    dot_general x6, matrix products, product(): jnp.dot(rows[0], mine, preferred_element_type=jnp.float32)  14.1 us
    dot_general x2, matrix products, chan_terms(): terms = jnp.dot(hidden, down_full, preferred_element_type=jnp.float32)  11.4 us
    ppermute x15, starting transfers between devices, swap(): return lax.ppermute(x, axis, [(0, 1), (1, 0)])  9.9 us
  transfers between devices with their start and end apart: 25, of which 12 were waited for; matrix products, arithmetic and copies ran while one was open for 23% of the time, Pallas kernels for 0%

profile of v1, /device:TPU:0, one launch (start us, length us, event | category | flops | bytes accessed | tf_op | source)
XLA Modules:
  0.0 364.0 jit_solution(3442184704574350597)
XLA Ops:
  12.4 3.0 collective-permute-start.4
  21.7 10.2 %collective-permute-done.16 = bf16[1024,256]{1,0:T(8,128)(2,1)} collective-permute-done((bf16[1024,256]{1,0:T(8,128)(2,1)}, bf16[1024,256]{1,0:T(8,128)(2,1)}, u32[]{:S(2)}, u32[]{:S(2)}) %collective-permute-start.16) | collective-permute-done | bytes 524320 | tf_op jit(solution)/shard_map/ppermute | solution.py:61
  34.5 4.1 %collective-permute-done.4 = bf16[512,1024]{1,0:T(8,128)(2,1)S(1)} collective-permute-done((bf16[512,1024]{1,0:T(8,128)(2,1)S(1)}, bf16[512,1024]{1,0:T(8,128)(2,1)S(1)}, u32[]{:S(2)}, u32[]{:S(2)}) %collective-permute-start.4) | collective-permute-done | bytes 1048608 | tf_op jit(solution)/shard_map/ppermute | solution.py:38
  42.3 15.8 %all-gather.6.cloned.1.call-done = bf16[1024,1024]{1,0:T(8,128)(2,1)} async-done(((bf16[256,1024]{1,0:T(8,128)(2,1)}), bf16[1024,1024]{1,0:T(8,128)(2,1)}) %all-gather.6.cloned.1.call-update) | async-done | bytes 2097168 | tf_op jit(solution)/shard_map/all_gather | solution.py:57
  61.6 42.5 %all-gather.8.cloned.1.call-done = bf16[1024,1024]{1,0:T(8,128)(2,1)} async-done(((bf16[256,1024]{1,0:T(8,128)(2,1)}), bf16[1024,1024]{1,0:T(8,128)(2,1)}) %all-gather.8.cloned.1.call-update) | async-done | bytes 2097168 | tf_op jit(solution)/shard_map/all_gather | solution.py:57
  105.6 45.2 %all-gather.10.cloned.1.call-done = bf16[1024,1024]{1,0:T(8,128)(2,1)} async-done(((bf16[1024,256]{1,0:T(8,128)(2,1)}), bf16[1024,1024]{1,0:T(8,128)(2,1)}) %all-gather.10.cloned.1.call-update) | async-done | bytes 2097168 | tf_op jit(solution)/shard_map/all_gather | solution.py:57
  152.3 3.4 fusion.226
  161.8 2.9 convolution_add_fusion
  167.1 2.9 convolution_add_fusion.1
  172.4 4.0 %add_convert_fusion.1 = bf16[512,1024]{1,0:T(8,128)(2,1)} fusion(f32[512,1024]{1,0:T(8,128)S(1)} %fusion.225, bf16[1024,1024]{1,0:T(8,128)(2,1)} %collective-permute-done.2, bf16[512,256]{1,0:T(8,128)(2,1)S(1)} %copy-done.15, bf16[512,256]{1,0:T(8,128)(2,1)S(1)} %copy-done.14, bf16[512,256]{1,0:T(8,128)(2,1)S(1)} %copy-done.13, ...), kind=kOutput, calls=%fused_computation.20 | convolution fusion | flops 1080557568 | bytes 6297600 | tf_op jit(solution)/shard_map/dot_general | solution.py:131
  176.3 4.4 %multiply_reduce_fusion.7 = (f32[512]{0:T(512)}, f32[512,512]{0,1:T(8,128)}) fusion(bf16[512,1024]{1,0:T(8,128)(2,1)} %add_convert_fusion.1, f32[]{:T(128)} %bitcast, f32[512]{0:T(512)S(1)} %iota_convert_fusion, f32[512,128]{1,0:T(8,128)} %get-tuple-element.25, f32[512,128]{1,0:T(8,128)} %get-tuple-element.24, bf16[512,128]{1,0:T(8,128)(2,1)} %get-tuple-element.26, ...), kind=kOutput, calls=%fused_computation.102 | convolution fusion | flops 405929472 | bytes 2365952 | tf_op jit(solution)/shard_map/dot_general | solution.py:168
  180.7 4.8 %add_convert_fusion.2 = bf16[512,1024]{1,0:T(8,128)(2,1)} fusion(f32[512,1024]{1,0:T(8,128)} %fusion.223, bf16[1024,1024]{1,0:T(8,128)(2,1)} %collective-permute-done.2, bf16[512,256]{1,0:T(8,128)(2,1)} %get-tuple-element.64, bf16[512,256]{1,0:T(8,128)(2,1)} %get-tuple-element.61, bf16[512,256]{1,0:T(8,128)(2,1)} %get-tuple-element.59, ...), kind=kOutput, calls=%fused_computation.25 | convolution fusion | flops 1080557568 | bytes 6297600 | tf_op jit(solution)/shard_map/dot_general | solution.py:131
  185.5 4.4 %multiply_reduce_fusion.9 = (f32[512]{0:T(512)}, f32[512,512]{0,1:T(8,128)}) fusion(bf16[512,1024]{1,0:T(8,128)(2,1)} %add_convert_fusion.2, f32[]{:T(128)} %bitcast, f32[512]{0:T(512)S(1)} %iota_convert_fusion, f32[512,128]{1,0:T(8,128)} %get-tuple-element.17, f32[512,128]{1,0:T(8,128)} %get-tuple-element.16, bf16[512,128]{1,0:T(8,128)(2,1)} %get-tuple-element.18, ...), kind=kOutput, calls=%fused_computation.107 | convolution fusion | flops 405929472 | bytes 2365952 | tf_op jit(solution)/shard_map/dot_general | solution.py:168
  190.5 4.2 %multiply_reduce_fusion.6 = (f32[512]{0:T(512)}, f32[512,512]{0,1:T(8,128)}) fusion(bf16[512,1024]{1,0:T(8,128)(2,1)} %add_convert_fusion.1, f32[]{:T(128)} %bitcast.2, f32[512]{0:T(512)S(1)} %iota_convert_fusion, f32[512,128]{1,0:T(8,128)} %get-tuple-element.21, f32[512,128]{1,0:T(8,128)S(1)} %copy-done.23, bf16[512,128]{1,0:T(8,128)(2,1)} %get-tuple-element.23, ...), kind=kOutput, calls=%fused_computation.100 | convolution fusion | flops 405929472 | bytes 2365952 | tf_op jit(solution)/shard_map/dot_general | solution.py:168
  195.5 3.8 %multiply_reduce_fusion.8 = (f32[512]{0:T(512)S(1)}, f32[512,512]{0,1:T(8,128)}) fusion(bf16[512,1024]{1,0:T(8,128)(2,1)} %add_convert_fusion.2, f32[]{:T(128)} %bitcast.2, f32[512]{0:T(512)S(1)} %iota_convert_fusion, f32[512,128]{1,0:T(8,128)} %get-tuple-element.13, f32[512,128]{1,0:T(8,128)} %get-tuple-element.12, ...), kind=kOutput, calls=%fused_computation.105 | convolution fusion | flops 405929472 | bytes 2365952 | tf_op jit(solution)/shard_map/dot_general | solution.py:168
  211.0 12.5 %collective-permute-done.11 = bf16[512,512]{1,0:T(8,128)(2,1)S(1)} collective-permute-done((bf16[512,512]{1,0:T(8,128)(2,1)S(1)}, bf16[512,512]{1,0:T(8,128)(2,1)S(1)}, u32[]{:S(2)}, u32[]{:S(2)}) %collective-permute-start.11) | collective-permute-done | bytes 524320 | tf_op jit(solution)/shard_map/ppermute | solution.py:38
  223.5 10.7 %collective-permute-done.7 = bf16[512,512]{1,0:T(8,128)(2,1)S(1)} collective-permute-done((bf16[512,512]{1,0:T(8,128)(2,1)S(1)}, bf16[512,512]{1,0:T(8,128)(2,1)S(1)}, u32[]{:S(2)}, u32[]{:S(2)}) %collective-permute-start.7) | collective-permute-done | bytes 524320 | tf_op jit(solution)/shard_map/ppermute | solution.py:38
  236.7 23.3 %collective-permute-done.14 = bf16[512,1024]{1,0:T(8,128)(2,1)S(1)} collective-permute-done((bf16[512,1024]{1,0:T(8,128)(2,1)S(1)}, bf16[512,1024]{1,0:T(8,128)(2,1)S(1)}, u32[]{:S(2)}, u32[]{:S(2)}) %collective-permute-start.14) | collective-permute-done | bytes 1048608 | tf_op jit(solution)/shard_map/ppermute | solution.py:38
  267.2 2.6 fusion.23
  269.8 38.5 %collective-permute-done.13 = bf16[1024,1024]{1,0:T(8,128)(2,1)} collective-permute-done((bf16[1024,1024]{1,0:T(8,128)(2,1)}, bf16[1024,1024]{1,0:T(8,128)(2,1)}, u32[]{:S(2)}, u32[]{:S(2)}) %collective-permute-start.13) | collective-permute-done | bytes 2097184 | tf_op jit(solution)/shard_map/ppermute | solution.py:61
  308.4 9.0 %fusion.60 = f32[512,2048]{1,0:T(8,128)} fusion(bf16[1024,2048]{1,0:T(8,128)(2,1)} %all-gather.14.cloned.1.call-done, f32[512,1024]{1,0:T(8,128)} %fusion.23, bf16[1024,1024]{1,0:T(8,128)(2,1)} %collective-permute-done.13, bf16[512,256]{1,0:T(8,128)(2,1)S(1)} %get-tuple-element.50, bf16[512,256]{1,0:T(8,128)(2,1)S(1)} %get-tuple-element.47, ...), kind=kOutput, calls=%fused_computation.116 | convolution fusion | flops 3229089792 | bytes 13637632 | tf_op jit(solution)/shard_map/dot_general | solution.py:187
  319.4 2.9 fusion.22
  322.3 3.1 multiply_convert_fusion.3
  332.9 22.9 %collective-permute-done.19 = bf16[512,1024]{1,0:T(8,128)(2,1)S(1)} collective-permute-done((bf16[512,1024]{1,0:T(8,128)(2,1)S(1)}, bf16[512,1024]{1,0:T(8,128)(2,1)S(1)}, u32[]{:S(2)}, u32[]{:S(2)}) %collective-permute-start.19) | collective-permute-done | bytes 1048608 | tf_op jit(solution)/shard_map/ppermute | solution.py:38
  (203 shorter events, 69.0 us)
Async XLA Ops:
  6.5 51.5 %all-gather.6.cloned.1.call-start = ((), (), s32[]{:S(2)}) async-start(), calls=%async_computation | async-start | bytes 2621440 | tf_op jit(solution)/shard_map/all_gather | solution.py:57
  9.5 94.6 %all-gather.8.cloned.1.call-start = ((), (), s32[]{:S(2)}) async-start(), calls=%async_computation.1 | async-start | bytes 2621440 | tf_op jit(solution)/shard_map/all_gather | solution.py:57
  10.5 140.3 %all-gather.10.cloned.1.call-start = ((), (), s32[]{:S(2)}) async-start(), calls=%async_computation.2 | async-start | bytes 2621440 | tf_op jit(solution)/shard_map/all_gather | solution.py:57
  11.4 248.5 %all-gather.12.cloned.1.call-start = ((), (), s32[]{:S(2)}) async-start(), calls=%async_computation.3 | async-start | bytes 2621440 | tf_op jit(solution)/shard_map/all_gather | solution.py:57
  12.4 296.0 %all-gather.14.cloned.1.call-start = ((), (), s32[]{:S(2)}) async-start(), calls=%async_computation.4 | async-start | bytes 5242880 | tf_op jit(solution)/shard_map/all_gather | solution.py:57
  12.4 26.2 %collective-permute-start.4 = (bf16[512,1024]{1,0:T(8,128)(2,1)S(1)}, bf16[512,1024]{1,0:T(8,128)(2,1)S(1)}, u32[]{:S(2)}, u32[]{:S(2)}) collective-permute-start(bf16[512,1024]{1,0:T(8,128)(2,1)S(1)} %copy-done.2), channel_id=1, source_target_pairs={{0,16},{16,0},{1,17},{17,1},{2,18},{18,2},{3,19},{19,3},{4,20},{20... | collective-permute-start | bytes 3145736 | tf_op jit(solution)/shard_map/ppermute | solution.py:38
  15.4 23.4 %collective-permute-start = (bf16[512,1024]{1,0:T(8,128)(2,1)S(1)}, bf16[512,1024]{1,0:T(8,128)(2,1)S(1)}, u32[]{:S(2)}, u32[]{:S(2)}) collective-permute-start(bf16[512,1024]{1,0:T(8,128)(2,1)S(1)} %copy-done.2), channel_id=1, source_target_pairs={{0,1},{1,0},{2,3},{3,2},{4,5},{5,4},{6,7},{7,6},{8,9},{9,8},{10,11... | collective-permute-start | bytes 3145736 | tf_op jit(solution)/shard_map/ppermute | solution.py:38
  17.3 14.7 %collective-permute-start.16 = (bf16[1024,256]{1,0:T(8,128)(2,1)}, bf16[1024,256]{1,0:T(8,128)(2,1)}, u32[]{:S(2)}, u32[]{:S(2)}) collective-permute-start(bf16[1024,256]{1,0:T(8,128)(2,1)} %constant_dynamic-slice_fusion.1), channel_id=1, source_target_pairs={{0,2},{2,0},{4,6},{6,4},{8,10},{10,8},{12,14},{14,12},{1,3},{3,1},... | collective-permute-start | bytes 1572872 | tf_op jit(solution)/shard_map/ppermute | solution.py:61
  38.6 2.9 collective-permute-start.5
  58.1 103.7 %collective-permute-start.1 = (bf16[1024,1024]{1,0:T(8,128)(2,1)}, bf16[1024,1024]{1,0:T(8,128)(2,1)}, u32[]{:S(2)}, u32[]{:S(2)}) collective-permute-start(bf16[1024,1024]{1,0:T(8,128)(2,1)} %all-gather.6.cloned.1.call-done), channel_id=1, source_target_pairs={{0,2},{2,0},{4,6},{6,4},{8,10},{10,8},{12,14},{14,12},{1,3},{3,1},... | collective-permute-start | bytes 6291464 | tf_op jit(solution)/shard_map/ppermute | solution.py:61
  104.1 68.2 %collective-permute-start.2 = (bf16[1024,1024]{1,0:T(8,128)(2,1)}, bf16[1024,1024]{1,0:T(8,128)(2,1)}, u32[]{:S(2)}, u32[]{:S(2)}) collective-permute-start(bf16[1024,1024]{1,0:T(8,128)(2,1)} %all-gather.8.cloned.1.call-done), channel_id=1, source_target_pairs={{0,2},{2,0},{4,6},{6,4},{8,10},{10,8},{12,14},{14,12},{1,3},{3,1},... | collective-permute-start | bytes 6291464 | tf_op jit(solution)/shard_map/ppermute | solution.py:61
  150.8 50.8 %collective-permute-start.8 = (bf16[1024,1024]{1,0:T(8,128)(2,1)}, bf16[1024,1024]{1,0:T(8,128)(2,1)S(1)}, u32[]{:S(2)}, u32[]{:S(2)}) collective-permute-start(bf16[1024,1024]{1,0:T(8,128)(2,1)} %all-gather.10.cloned.1.call-done), channel_id=1, source_target_pairs={{0,2},{2,0},{4,6},{6,4},{8,10},{10,8},{12,14},{14,12},{1,3},{3,1},... | collective-permute-start | bytes 6291464 | tf_op jit(solution)/shard_map/ppermute | solution.py:61
  203.0 8.0 %collective-permute-start.9 = (bf16[512,512]{1,0:T(8,128)(2,1)S(1)}, bf16[512,512]{1,0:T(8,128)(2,1)S(1)}, u32[]{:S(2)}, u32[]{:S(2)}) collective-permute-start(bf16[512,512]{1,0:T(8,128)(2,1)S(1)} %dynamic-slice_convert_fusion.3), channel_id=1, source_target_pairs={{0,1},{1,0},{2,3},{3,2},{4,5},{5,4},{6,7},{7,6},{8,9},{9,8},{10,11... | collective-permute-start | bytes 1572872 | tf_op jit(solution)/shard_map/ppermute | solution.py:38
  204.5 4.0 %collective-permute-start.10 = (bf16[512,512]{1,0:T(8,128)(2,1)S(1)}, bf16[512,512]{1,0:T(8,128)(2,1)S(1)}, u32[]{:S(2)}, u32[]{:S(2)}) collective-permute-start(bf16[512,512]{1,0:T(8,128)(2,1)S(1)} %dynamic-slice_convert_fusion.2), channel_id=1, source_target_pairs={{0,1},{1,0},{2,3},{3,2},{4,5},{5,4},{6,7},{7,6},{8,9},{9,8},{10,11... | collective-permute-start | bytes 1572872 | tf_op jit(solution)/shard_map/ppermute | solution.py:38
  206.5 3.7 %collective-permute-start.6 = (bf16[512,512]{1,0:T(8,128)(2,1)S(1)}, bf16[512,512]{1,0:T(8,128)(2,1)S(1)}, u32[]{:S(2)}, u32[]{:S(2)}) collective-permute-start(bf16[512,512]{1,0:T(8,128)(2,1)S(1)} %dynamic-slice_convert_fusion.4), channel_id=1, source_target_pairs={{0,1},{1,0},{2,3},{3,2},{4,5},{5,4},{6,7},{7,6},{8,9},{9,8},{10,11... | collective-permute-start | bytes 1572872 | tf_op jit(solution)/shard_map/ppermute | solution.py:38
  208.7 14.9 %collective-permute-start.11 = (bf16[512,512]{1,0:T(8,128)(2,1)S(1)}, bf16[512,512]{1,0:T(8,128)(2,1)S(1)}, u32[]{:S(2)}, u32[]{:S(2)}) collective-permute-start(bf16[512,512]{1,0:T(8,128)(2,1)S(1)} %add_convert_fusion.3), channel_id=1, source_target_pairs={{0,16},{16,0},{1,17},{17,1},{2,18},{18,2},{3,19},{19,3},{4,20},{20... | collective-permute-start | bytes 1572872 | tf_op jit(solution)/shard_map/ppermute | solution.py:38
  210.3 23.9 %collective-permute-start.7 = (bf16[512,512]{1,0:T(8,128)(2,1)S(1)}, bf16[512,512]{1,0:T(8,128)(2,1)S(1)}, u32[]{:S(2)}, u32[]{:S(2)}) collective-permute-start(bf16[512,512]{1,0:T(8,128)(2,1)S(1)} %add_convert_fusion.4), channel_id=1, source_target_pairs={{0,16},{16,0},{1,17},{17,1},{2,18},{18,2},{3,19},{19,3},{4,20},{20... | collective-permute-start | bytes 1572872 | tf_op jit(solution)/shard_map/ppermute | solution.py:38
  235.2 24.8 %collective-permute-start.14 = (bf16[512,1024]{1,0:T(8,128)(2,1)S(1)}, bf16[512,1024]{1,0:T(8,128)(2,1)S(1)}, u32[]{:S(2)}, u32[]{:S(2)}) collective-permute-start(bf16[512,1024]{1,0:T(8,128)(2,1)S(1)} %get-tuple-element.8), channel_id=1, source_target_pairs={{0,16},{16,0},{1,17},{17,1},{2,18},{18,2},{3,19},{19,3},{4,20},{20... | collective-permute-start | bytes 3145736 | tf_op jit(solution)/shard_map/ppermute | solution.py:38
  236.6 24.2 %collective-permute-start.12 = (bf16[512,1024]{1,0:T(8,128)(2,1)S(1)}, bf16[512,1024]{1,0:T(8,128)(2,1)S(1)}, u32[]{:S(2)}, u32[]{:S(2)}) collective-permute-start(bf16[512,1024]{1,0:T(8,128)(2,1)S(1)} %get-tuple-element.8), channel_id=1, source_target_pairs={{0,1},{1,0},{2,3},{3,2},{4,5},{5,4},{6,7},{7,6},{8,9},{9,8},{10,11... | collective-permute-start | bytes 3145736 | tf_op jit(solution)/shard_map/ppermute | solution.py:38
  259.9 2.8 collective-permute-start.15
  260.0 48.4 %collective-permute-start.13 = (bf16[1024,1024]{1,0:T(8,128)(2,1)}, bf16[1024,1024]{1,0:T(8,128)(2,1)}, u32[]{:S(2)}, u32[]{:S(2)}) collective-permute-start(bf16[1024,1024]{1,0:T(8,128)(2,1)} %all-gather.12.cloned.1.call-done), channel_id=1, source_target_pairs={{0,2},{2,0},{4,6},{6,4},{8,10},{10,8},{12,14},{14,12},{1,3},{3,1},... | collective-permute-start | bytes 6291464 | tf_op jit(solution)/shard_map/ppermute | solution.py:61
  319.2 6.1 %collective-permute-start.17 = (bf16[512,1024]{1,0:T(8,128)(2,1)S(1)}, bf16[512,1024]{1,0:T(8,128)(2,1)S(1)}, u32[]{:S(2)}, u32[]{:S(2)}) collective-permute-start(bf16[512,1024]{1,0:T(8,128)(2,1)S(1)} %dynamic-slice_convert_fusion.1), channel_id=1, source_target_pairs={{0,1},{1,0},{2,3},{3,2},{4,5},{5,4},{6,7},{7,6},{8,9},{9,8},{10,11... | collective-permute-start | bytes 3145736 | tf_op jit(solution)/shard_map/ppermute | solution.py:38
  330.1 2.8 collective-permute-start.18
  330.6 25.1 %collective-permute-start.19 = (bf16[512,1024]{1,0:T(8,128)(2,1)S(1)}, bf16[512,1024]{1,0:T(8,128)(2,1)S(1)}, u32[]{:S(2)}, u32[]{:S(2)}) collective-permute-start(bf16[512,1024]{1,0:T(8,128)(2,1)S(1)} %add_convert_fusion), channel_id=1, source_target_pairs={{0,16},{16,0},{1,17},{17,1},{2,18},{18,2},{3,19},{19,3},{4,20},{20... | collective-permute-start | bytes 3145736 | tf_op jit(solution)/shard_map/ppermute | solution.py:38
  (45 other events, 381.5 us)
Sparse Core Ops, SparseCore 0:
  9.7 48.3 all-gather.5
  59.6 44.4 all-gather.7
  105.7 45.0 all-gather.9
  152.2 43.8 all-gather.11
  197.5 79.5 all-gather.13
